TPU v7x, 32 devices: a whole 2x2x4 slice. The times are simulated.
32 devices in a mesh: grp: 2 (over y), sp: 4 (over z), tp: 4 (over x, core).
Axes of the slice: x: 2, y: 2, z: 4, core: 2. Of those that a mesh axis runs over, the one named last changes fastest.
Arguments:
- resid_in: bfloat16 [2048, 2048], P(('grp', 'sp', 'tp')), parts along dimension 0, may hold values from -3 to 3
- queries: bfloat16 [2048, 1024], P(('grp', 'sp'), 'tp'), parts along dimension 0, may hold values from -39 to 39
- keys: bfloat16 [2048, 1024], P(('grp', 'sp'), 'tp'), parts along dimension 0, may hold values from -6 to 6
- values: bfloat16 [2048, 1024], P(('grp', 'sp'), 'tp'), parts along dimension 0, may hold values from -12 to 12
- cum_gate: float32 [2048, 16], P('grp', 'tp'), parts along dimension 0, may hold values from -105 to 0, as said below
- w_out: bfloat16 [1024, 2048], replicated, may hold values from -0.1875 to 0.1875
- norm_gain: float32 [2048], replicated, may hold values from 0.1 to 1.9
- w_gate: bfloat16 [2048, 5632], P('sp', 'tp'), may hold values from -0.125 to 0.125
- w_up: bfloat16 [2048, 5632], P('sp', 'tp'), may hold values from -0.125 to 0.125
- w_down: bfloat16 [5632, 2048], P('tp', 'sp'), may hold values from -0.078125 to 0.078125
Outputs:
- resid_out: bfloat16 [2048, 2048], P(('grp', 'sp', 'tp')), parts along dimension 0
There are 2 independent parts, one for each index of `grp`. A program takes and returns all parts, laid end to end along the dimension named above; an argument that names none is the same for every part. Nothing has to cross between parts.
Inputs may be any that keep to these rules, and one draw needn't show every extreme that they name: `cum_gate`: in every head the values never rise from one position to the next, and the first is at most 0.
All inputs are finite; a program needn't handle non-finite values.
Results may differ from a plain program's by a relative error of at most 0.018.
Values may be sent and summed in bfloat16 or wider, within the bound.
A program may use at most 128 MiB of HBM per device.

v0:
```python
import math
import jax
import jax.numpy as jnp
from jax import lax
from jax.sharding import PartitionSpec as P

HEAD_DIM = 64


def on_device(resid_in, queries, keys, values, cum_gate, w_out, norm_gain, w_gate, w_up, w_down):
    tok_rows = queries.shape[0]
    local_heads = queries.shape[1] // HEAD_DIM
    scale = HEAD_DIM ** (-0.5)
    offset = lax.axis_index("sp") * tok_rows
    query_heads = queries.reshape(tok_rows, local_heads, HEAD_DIM)
    own_gate = lax.dynamic_slice_in_dim(cum_gate, offset, tok_rows, 0).T
    query_pos = offset + jnp.arange(tok_rows, dtype=jnp.int32)
    last_pos = offset + tok_rows - 1
    initial = (
        jnp.full((local_heads, tok_rows), -1e30, jnp.float32),
        jnp.zeros((local_heads, tok_rows), jnp.float32),
        jnp.zeros((tok_rows, local_heads, HEAD_DIM), jnp.float32),
    )
    key_piece = lax.all_gather(keys, "sp", axis=0, tiled=True)
    value_piece = lax.all_gather(values, "sp", axis=0, tiled=True)
    length = key_piece.shape[0]
    span = math.gcd(length, 512)

    def block(index, state):
        begin = index * span

        def work(inner):
            maxima, totals, summed = inner
            key_block = lax.dynamic_slice_in_dim(key_piece, index * span, span, 0).reshape(
                span, local_heads, HEAD_DIM
            )
            value_block_rows = lax.dynamic_slice_in_dim(value_piece, index * span, span, 0).reshape(
                span, local_heads, HEAD_DIM
            )
            key_gate = lax.dynamic_slice_in_dim(cum_gate, begin, span, 0).T
            scores = (
                jnp.einsum(
                    "qhd,khd->hqk", query_heads, key_block, preferred_element_type=jnp.float32
                )
                * scale
            )
            scores = scores + own_gate[:, :, None] - key_gate[:, None, :]
            key_pos = begin + jnp.arange(span, dtype=jnp.int32)
            mask = (key_pos[None, :] <= query_pos[:, None])[None]
            scores = jnp.where(mask, scores, -1e30)
            new_max = jnp.maximum(maxima, jnp.max(scores, axis=-1))
            weights = jnp.where(mask, jnp.exp(scores - new_max[:, :, None]), 0.0)
            rescale = jnp.exp(maxima - new_max)
            totals = totals * rescale + jnp.sum(weights, axis=-1)
            product = jnp.einsum(
                "hqk,khd->qhd",
                weights.astype(jnp.bfloat16),
                value_block_rows,
                preferred_element_type=jnp.float32,
            )
            summed = summed * rescale.T[:, :, None] + product
            return (new_max, totals, summed)

        return lax.cond(begin <= last_pos, work, lambda inner: inner, state)

    maxima, totals, summed = lax.fori_loop(0, length // span, block, initial)
    attended = (
        (summed / totals.T[:, :, None])
        .reshape(tok_rows, local_heads * HEAD_DIM)
        .astype(jnp.bfloat16)
    )
    head_rows = lax.all_to_all(attended, "tp", split_axis=0, concat_axis=1, tiled=True)
    mixed = jnp.dot(head_rows, w_out, preferred_element_type=jnp.float32)
    resid = resid_in.astype(jnp.float32) + mixed
    normed = resid * lax.rsqrt(jnp.mean(resid * resid, axis=-1, keepdims=True) + 1e-06)
    normed = (normed * norm_gain).astype(jnp.bfloat16)
    all_rows = lax.all_gather(normed, "tp", axis=0, tiled=True)
    full_gate, full_up, full_down = (
        lax.all_gather(w_gate, "sp", axis=0, tiled=True),
        lax.all_gather(w_up, "sp", axis=0, tiled=True),
        lax.all_gather(w_down, "sp", axis=1, tiled=True),
    )
    gate = jnp.dot(all_rows, full_gate, preferred_element_type=jnp.float32)
    up = jnp.dot(all_rows, full_up, preferred_element_type=jnp.float32)
    hidden = (jax.nn.silu(gate) * up).astype(jnp.bfloat16)
    terms = jnp.dot(hidden, full_down, preferred_element_type=jnp.float32)
    back = lax.psum_scatter(
        terms.astype(jnp.bfloat16), "tp", scatter_dimension=0, tiled=True
    ).astype(jnp.float32)
    return (resid + back).astype(jnp.bfloat16)


def solution(mesh):
    return jax.shard_map(
        on_device,
        mesh=mesh,
        in_specs=(
            P(("grp", "sp", "tp"), None),
            P(("grp", "sp"), "tp"),
            P(("grp", "sp"), "tp"),
            P(("grp", "sp"), "tp"),
            P("grp", "tp"),
            P(),
            P(),
            P("sp", "tp"),
            P("sp", "tp"),
            P("tp", "sp"),
        ),
        out_specs=P(("grp", "sp", "tp"), None),
        check_vma=False,
    )
```

profile of v0, /device:TPU:0, one launch (start us, length us, event | category | flops | bytes accessed | tf_op | source)
XLA Modules:
  0.0 436.8 jit_solution(10608171273558845246)
XLA Ops:
  6.5 0.0 copy-start.1
  6.5 0.0 all-gather.5.cloned.1.call-start
  6.5 1.0 copy.16
  7.6 17.4 %all_gather.18 = bf16[1024,256]{0,1:T(8,128)(2,1)S(1)} all-gather(bf16[256,256]{0,1:T(8,128)(2,1)S(1)} %copy.16), channel_id=1, replica_groups=mesh['grp'=2,'sp'=4,'tp'=4] {'sp'}, dimensions={0}, use_global_device_ids=true | all-gather | bytes 655360 | tf_op jit(solution)/shard_map/all_gather | solution.py:24
  24.9 1.0 copy.18
  25.9 16.3 %all_gather.19 = bf16[1024,256]{0,1:T(8,128)(2,1)S(1)} all-gather(bf16[256,256]{0,1:T(8,128)(2,1)S(1)} %copy.18), channel_id=1, replica_groups=mesh['grp'=2,'sp'=4,'tp'=4] {'sp'}, dimensions={0}, use_global_device_ids=true | all-gather | bytes 655360 | tf_op jit(solution)/shard_map/all_gather | solution.py:25
  42.2 1.0 copy.17
  43.2 0.0 copy-done.1
  43.3 0.0 copy-start
  43.3 2.1 while.18
  43.3 2.0 conditional.3
  43.4 0.1 broadcast_compare_fusion
  43.6 0.7 fusion.13
  44.3 0.5 fusion.4
  44.9 0.4 fusion.3
  45.4 0.2 reshape.60
  45.6 0.2 copy.22
  45.7 7.2 %all_to_all.16 = bf16[4,64,256]{2,1,0:T(8,128)(2,1)S(1)} all-to-all(bf16[4,64,256]{2,1,0:T(8,128)(2,1)S(1)} %copy.22), channel_id=1, replica_groups=mesh['grp'=2,'sp'=4,'tp'=4] {'tp'}, dimensions={0} | all-to-all | bytes 262144 | tf_op jit(solution)/shard_map/all_to_all | solution.py:72
  52.9 0.0 copy-done
  52.9 0.0 copy-start.2
  52.9 3.2 multiply_reduce_fusion
  56.1 0.0 copy-done.2
  56.1 0.8 multiply_convert_fusion
  56.9 0.0 all-gather.5.cloned.1.call-update
  57.0 0.0 all-gather.7.cloned.1.call-start
  57.0 0.7 all-gather.7.cloned.1.call-update
  57.7 0.0 all-gather.11.cloned.1.call-start
  57.8 0.7 all-gather.11.cloned.1.call-update
  58.5 0.0 all-gather.9.cloned.1.call-start
  58.5 0.5 all-gather.9.cloned.1.call-update
  59.0 0.0 reduce-scatter.2.cloned.1.call-start
  59.1 16.3 %all-gather.5.cloned.1.call-done = bf16[256,2048]{1,0:T(8,128)(2,1)} async-done(((bf16[64,2048]{1,0:T(8,128)(2,1)}), bf16[256,2048]{1,0:T(8,128)(2,1)}) %all-gather.5.cloned.1.call-update) | async-done | bytes 1048592 | tf_op jit(solution)/shard_map/all_gather | solution.py:77
  75.3 0.0 copy-start.3
  75.3 108.3 %all-gather.7.cloned.1.call-done = bf16[2048,1408]{1,0:T(8,128)(2,1)} async-done(((bf16[512,1408]{1,0:T(8,128)(2,1)}), bf16[2048,1408]{1,0:T(8,128)(2,1)}) %all-gather.7.cloned.1.call-update) | async-done | bytes 5767184 | tf_op jit(solution)/shard_map/all_gather | solution.py:79
  183.6 4.8 %fusion.14 = f32[256,1408]{1,0:T(8,128)S(1)} fusion(bf16[256,2048]{1,0:T(8,128)(2,1)} %all-gather.5.cloned.1.call-done, bf16[2048,1408]{1,0:T(8,128)(2,1)} %all-gather.7.cloned.1.call-done), kind=kOutput, calls=%fused_computation.32 | convolution fusion | flops 1476395008 | bytes 8257536 | tf_op jit(solution)/shard_map/dot_general | solution.py:83
  188.4 101.8 %all-gather.11.cloned.1.call-done = bf16[1408,2048]{1,0:T(8,128)(2,1)} async-done(((bf16[1408,512]{1,0:T(8,128)(2,1)}), bf16[1408,2048]{1,0:T(8,128)(2,1)}) %all-gather.11.cloned.1.call-update) | async-done | bytes 5767184 | tf_op jit(solution)/shard_map/all_gather | solution.py:81
  290.2 106.4 %all-gather.9.cloned.1.call-done = bf16[2048,1408]{1,0:T(8,128)(2,1)} async-done(((bf16[512,1408]{1,0:T(8,128)(2,1)}), bf16[2048,1408]{1,0:T(8,128)(2,1)}) %all-gather.9.cloned.1.call-update) | async-done | bytes 5767184 | tf_op jit(solution)/shard_map/all_gather | solution.py:80
  396.6 0.0 copy-done.3
  396.6 8.8 %convolution_convert_fusion = bf16[256,2048]{1,0:T(8,128)(2,1)} fusion(bf16[1408,2048]{1,0:T(8,128)(2,1)} %all-gather.11.cloned.1.call-done, bf16[256,2048]{1,0:T(8,128)(2,1)S(1)} %copy-done.3, bf16[2048,1408]{1,0:T(8,128)(2,1)} %all-gather.9.cloned.1.call-done, f32[256,1408]{1,0:T(8,128)S(1)} %fusion.14), kind=kOutput, calls=%fused_computation.22 | convolution fusion | flops 2955476992 | bytes 15073280 | tf_op jit(solution)/shard_map/dot_general | solution.py:86
  405.4 0.0 reduce-scatter.2.cloned.1.call-update
  405.4 23.2 %reduce-scatter.2.cloned.1.call-done = bf16[64,2048]{1,0:T(8,128)(2,1)} async-done(((bf16[256,2048]{1,0:T(8,128)(2,1)}), bf16[64,2048]{1,0:T(8,128)(2,1)}) %reduce-scatter.2.cloned.1.call-update) | async-done | bytes 262160 | tf_op jit(solution)/shard_map/reduce_scatter | solution.py:87
  428.6 1.7 add_convert_fusion
  (17 shorter events, 0.2 us)
Async XLA Ops:
  6.5 36.7 %copy-start.1 = (f32[1024,4]{0,1:T(4,128)S(1)}, f32[1024,4]{0,1:T(4,128)}, u32[]{:S(2)}) copy-start(f32[1024,4]{0,1:T(4,128)} %param.18) | copy-start | bytes 49156
  6.5 68.8 %all-gather.5.cloned.1.call-start = ((), (), s32[]{:S(2)}) async-start(), calls=%async_computation.2 | async-start | bytes 1310720 | tf_op jit(solution)/shard_map/all_gather | solution.py:77
  43.3 9.6 %copy-start = (bf16[64,2048]{1,0:T(8,128)(2,1)S(1)}, bf16[64,2048]{1,0:T(8,128)(2,1)}, u32[]{:S(2)}) copy-start(bf16[64,2048]{1,0:T(8,128)(2,1)} %param.14) | copy-start | bytes 786436
  52.9 3.2 copy-start.2
  57.0 126.7 %all-gather.7.cloned.1.call-start = ((), (), s32[]{:S(2)}) async-start(), calls=%async_computation.3 | async-start | bytes 7208960 | tf_op jit(solution)/shard_map/all_gather | solution.py:79
  57.7 232.5 %all-gather.11.cloned.1.call-start = ((), (), s32[]{:S(2)}) async-start(), calls=%async_computation.5 | async-start | bytes 7208960 | tf_op jit(solution)/shard_map/all_gather | solution.py:81
  58.5 338.1 %all-gather.9.cloned.1.call-start = ((), (), s32[]{:S(2)}) async-start(), calls=%async_computation.4 | async-start | bytes 7208960 | tf_op jit(solution)/shard_map/all_gather | solution.py:80
  59.0 369.6 %reduce-scatter.2.cloned.1.call-start = ((), (), s32[]{:S(2)}) async-start(), calls=%async_computation.6 | async-start | bytes 1310720 | tf_op jit(solution)/shard_map/reduce_scatter | solution.py:87
  75.3 321.2 %copy-start.3 = (bf16[256,2048]{1,0:T(8,128)(2,1)S(1)}, bf16[256,2048]{1,0:T(8,128)(2,1)}, u32[]{:S(2)}) copy-start(bf16[256,2048]{1,0:T(8,128)(2,1)} %all-gather.5.cloned.1.call-done) | copy-start | bytes 3145732
Sparse Core Ops, SparseCore 0:
  57.1 18.2 all-gather.4
  76.9 106.6 all-gather.6
  185.2 104.9 all-gather.10
  291.6 104.9 all-gather.8
  405.5 23.0 reduce-scatter.1
where the time goes:
time: 437 us
  waiting for transfers between devices  358 us (82%)
  blocking collectives  40.8 us (9%)
  matrix products  18 us (4%)
  between operations  13.3 us (3%)
    all_gather x1, waiting for transfers between devices, on_device(): lax.all_gather(w_gate, 'sp', axis=0, tiled=True)  108 us
    all_gather x1, waiting for transfers between devices, on_device(): lax.all_gather(w_up, 'sp', axis=0, tiled=True)  106 us
    all_gather x1, waiting for transfers between devices, on_device(): lax.all_gather(w_down, 'sp', axis=1, tiled=True)  102 us
    reduce_scatter x1, waiting for transfers between devices, on_device(): lax.psum_scatter(terms.astype(jnp.bfloat16), 'tp', scatter_dimension=0, t...  23.2 us
    all_gather x1, blocking collectives, on_device(): key_piece = lax.all_gather(keys, 'sp', axis=0, tiled=True)  17.4 us
    all_gather x1, waiting for transfers between devices, on_device(): all_rows = lax.all_gather(normed, 'tp', axis=0, tiled=True)  16.3 us
    all_gather x1, blocking collectives, on_device(): value_piece = lax.all_gather(values, 'sp', axis=0, tiled=True)  16.3 us
    dot_general x1, matrix products, on_device(): terms = jnp.dot(hidden, full_down, preferred_element_type=jnp.float32)  8.81 us
  transfers between devices with their start and end apart: 5, of which 5 were waited for; matrix products, arithmetic and copies ran while one was open for 1% of the time, Pallas kernels for 0%

commit v1 on v0

--- a/solution.py
+++ b/solution.py
@@ -5,6 +5,12 @@
 from jax.sharding import PartitionSpec as P
 
 HEAD_DIM = 64
+
+
+def gather_blocks(x, axis, dim):
+    parts = lax.all_gather(x, axis, axis=0, tiled=False)
+    full = jnp.concatenate(parts, axis=dim)
+    return full
 
 
 def on_device(resid_in, queries, keys, values, cum_gate, w_out, norm_gain, w_gate, w_up, w_down):
@@ -78,7 +84,7 @@
     full_gate, full_up, full_down = (
         lax.all_gather(w_gate, "sp", axis=0, tiled=True),
         lax.all_gather(w_up, "sp", axis=0, tiled=True),
-        lax.all_gather(w_down, "sp", axis=1, tiled=True),
+        gather_blocks(w_down, "sp", 1),
     )
     gate = jnp.dot(all_rows, full_gate, preferred_element_type=jnp.float32)
     up = jnp.dot(all_rows, full_up, preferred_element_type=jnp.float32)

time: 437 us -> 402 us (0.920)
  waiting for transfers between devices: 358 us -> 302 us
  blocking collectives: 40.8 us -> 52.5 us
  local copies, waits for them, and re-layouts: 3.45 us -> 11.8 us
    all_gather x1, waiting for transfers between devices: 102 us -> 58.1 us  [gather_blocks(): parts = lax.all_gather(x, axis, axis=0, tiled=False)]
    reshape x0 -> x1, local copies, waits for them, and re-layouts: none -> 8.32 us  [gather_blocks(): full = jnp.concatenate(parts, axis=dim)]
    all_gather x1, blocking collectives: 16.3 us -> 24.2 us  [on_device(): value_piece = lax.all_gather(values, 'sp', axis=0, tiled=True)]
    all_gather x1, waiting for transfers between devices: 16.3 us -> 9.05 us  [on_device(): all_rows = lax.all_gather(normed, 'tp', axis=0, tiled=True)]
    all_gather x1, waiting for transfers between devices: 106 us -> 102 us  [on_device(): lax.all_gather(w_up, 'sp', axis=0, tiled=True)]
  transfers between devices with their start and end apart: 5 -> 5, of which waited for: 5 -> 5; matrix products, arithmetic and copies ran while one was open for 1% -> 6% of each run, Pallas kernels for 0% -> 0%
where the time goes in v1:
time: 402 us; the launch traced here: 401 us
  waiting for transfers between devices  302 us (75%)
  blocking collectives  52.5 us (13%)
  matrix products  18 us (4%)
  between operations  13.3 us (3%)
  local copies, waits for them, and re-layouts  11.8 us (3%)
    all_gather x1, waiting for transfers between devices, on_device(): lax.all_gather(w_gate, 'sp', axis=0, tiled=True)  108 us
    all_gather x1, waiting for transfers between devices, on_device(): lax.all_gather(w_up, 'sp', axis=0, tiled=True)  102 us
    all_gather x1, waiting for transfers between devices, gather_blocks(): parts = lax.all_gather(x, axis, axis=0, tiled=False)  58.1 us
    all_gather x1, blocking collectives, on_device(): value_piece = lax.all_gather(values, 'sp', axis=0, tiled=True)  24.2 us
    reduce_scatter x1, waiting for transfers between devices, on_device(): lax.psum_scatter(terms.astype(jnp.bfloat16), 'tp', scatter_dimension=0, t...  23.2 us
    all_gather x1, blocking collectives, on_device(): key_piece = lax.all_gather(keys, 'sp', axis=0, tiled=True)  21.3 us
    all_gather x1, waiting for transfers between devices, on_device(): all_rows = lax.all_gather(normed, 'tp', axis=0, tiled=True)  9.05 us
    dot_general x1, matrix products, on_device(): terms = jnp.dot(hidden, full_down, preferred_element_type=jnp.float32)  8.77 us
  transfers between devices with their start and end apart: 5, of which 5 were waited for; matrix products, arithmetic and copies ran while one was open for 6% of the time, Pallas kernels for 0%

profile of v1, /device:TPU:0, one launch (start us, length us, event | category | flops | bytes accessed | tf_op | source)
XLA Modules:
  0.0 401.2 jit_solution(9746494457292121686)
XLA Ops:
  6.5 0.0 copy-start.1
  6.5 0.0 all-gather.12.cloned.1.call-start
  6.5 0.7 all-gather.12.cloned.1.call-update
  7.3 0.0 all-gather.6.cloned.1.call-start
  7.3 1.0 copy.22
  8.3 1.0 copy.24
  9.3 1.0 copy.23
  10.3 0.0 copy-done.1
  10.4 21.3 %all_gather.21 = bf16[1024,256]{0,1:T(8,128)(2,1)S(1)} all-gather(bf16[256,256]{0,1:T(8,128)(2,1)S(1)} %copy.22), channel_id=1, replica_groups=mesh['grp'=2,'sp'=4,'tp'=4] {'sp'}, dimensions={0}, use_global_device_ids=true | all-gather | bytes 655360 | tf_op jit(solution)/shard_map/all_gather | solution.py:30
  31.7 24.2 %all_gather.22 = bf16[1024,256]{0,1:T(8,128)(2,1)S(1)} all-gather(bf16[256,256]{0,1:T(8,128)(2,1)S(1)} %copy.24), channel_id=1, replica_groups=mesh['grp'=2,'sp'=4,'tp'=4] {'sp'}, dimensions={0}, use_global_device_ids=true | all-gather | bytes 655360 | tf_op jit(solution)/shard_map/all_gather | solution.py:31
  55.9 0.0 copy-start
  55.9 2.1 while.18
  56.0 2.0 conditional.3
  56.1 0.1 broadcast_compare_fusion
  56.2 0.7 fusion.13
  57.0 0.5 fusion.4
  57.5 0.4 fusion.3
  58.0 0.2 reshape.69
  58.2 0.2 copy.29
  58.4 7.0 %all_to_all.16 = bf16[4,64,256]{2,1,0:T(8,128)(2,1)S(1)} all-to-all(bf16[4,64,256]{2,1,0:T(8,128)(2,1)S(1)} %copy.29), channel_id=1, replica_groups=mesh['grp'=2,'sp'=4,'tp'=4] {'tp'}, dimensions={0} | all-to-all | bytes 262144 | tf_op jit(solution)/shard_map/all_to_all | solution.py:78
  65.4 0.0 copy-done
  65.4 0.0 copy-start.2
  65.4 3.2 multiply_reduce_fusion
  68.6 0.0 copy-done.2
  68.6 0.8 multiply_convert_fusion
  69.4 0.0 all-gather.6.cloned.1.call-update
  69.4 0.0 all-gather.8.cloned.1.call-start
  69.5 0.7 all-gather.8.cloned.1.call-update
  70.2 0.0 all-gather.10.cloned.1.call-start
  70.2 0.5 all-gather.10.cloned.1.call-update
  70.7 0.0 reduce-scatter.2.cloned.1.call-start
  70.8 58.1 %all-gather.12.cloned.1.call-done = bf16[5632,512]{1,0:T(8,128)(2,1)} async-done(((bf16[1408,512]{1,0:T(8,128)(2,1)}), bf16[5632,512]{1,0:T(8,128)(2,1)}) %all-gather.12.cloned.1.call-update) | async-done | bytes 5767184 | tf_op jit(solution)/shard_map/all_gather | solution.py:11
  128.9 8.3 %copy.27 = bf16[1408,4,512]{0,2,1:T(8,128)(2,1)} copy(bf16[1408,4,512]{2,0,1:T(8,128)(2,1)} %bitcast.37) | data formatting | bytes 11534336 | tf_op jit(solution)/shard_map/reshape | solution.py:12
  137.2 9.0 %all-gather.6.cloned.1.call-done = bf16[256,2048]{1,0:T(8,128)(2,1)} async-done(((bf16[64,2048]{1,0:T(8,128)(2,1)}), bf16[256,2048]{1,0:T(8,128)(2,1)}) %all-gather.6.cloned.1.call-update) | async-done | bytes 1048592 | tf_op jit(solution)/shard_map/all_gather | solution.py:83
  146.3 0.0 copy-start.3
  146.3 108.3 %all-gather.8.cloned.1.call-done = bf16[2048,1408]{1,0:T(8,128)(2,1)} async-done(((bf16[512,1408]{1,0:T(8,128)(2,1)}), bf16[2048,1408]{1,0:T(8,128)(2,1)}) %all-gather.8.cloned.1.call-update) | async-done | bytes 5767184 | tf_op jit(solution)/shard_map/all_gather | solution.py:85
  254.6 4.8 %fusion.14 = f32[256,1408]{1,0:T(8,128)S(1)} fusion(bf16[256,2048]{1,0:T(8,128)(2,1)} %all-gather.6.cloned.1.call-done, bf16[2048,1408]{1,0:T(8,128)(2,1)} %all-gather.8.cloned.1.call-done), kind=kOutput, calls=%fused_computation.32 | convolution fusion | flops 1476395008 | bytes 8257536 | tf_op jit(solution)/shard_map/dot_general | solution.py:89
  259.4 101.6 %all-gather.10.cloned.1.call-done = bf16[2048,1408]{1,0:T(8,128)(2,1)} async-done(((bf16[512,1408]{1,0:T(8,128)(2,1)}), bf16[2048,1408]{1,0:T(8,128)(2,1)}) %all-gather.10.cloned.1.call-update) | async-done | bytes 5767184 | tf_op jit(solution)/shard_map/all_gather | solution.py:86
  361.0 0.0 copy-done.3
  361.0 8.8 %convolution_convert_fusion = bf16[256,2048]{1,0:T(8,128)(2,1)} fusion(bf16[1408,2048]{0,1:T(8,128)(2,1)} %bitcast.38, bf16[256,2048]{1,0:T(8,128)(2,1)S(1)} %copy-done.3, bf16[2048,1408]{1,0:T(8,128)(2,1)} %all-gather.10.cloned.1.call-done, f32[256,1408]{1,0:T(8,128)S(1)} %fusion.14), kind=kOutput, calls=%fused_computation.22 | convolution fusion | flops 2955476992 | bytes 15073280 | tf_op jit(solution)/shard_map/dot_general | solution.py:92
  369.8 0.0 reduce-scatter.2.cloned.1.call-update
  369.8 23.2 %reduce-scatter.2.cloned.1.call-done = bf16[64,2048]{1,0:T(8,128)(2,1)} async-done(((bf16[256,2048]{1,0:T(8,128)(2,1)}), bf16[64,2048]{1,0:T(8,128)(2,1)}) %reduce-scatter.2.cloned.1.call-update) | async-done | bytes 262160 | tf_op jit(solution)/shard_map/reduce_scatter | solution.py:93
  393.0 1.7 add_convert_fusion
  (17 shorter events, 0.2 us)
Async XLA Ops:
  6.5 3.8 copy-start.1
  6.5 122.4 %all-gather.12.cloned.1.call-start = ((), (), s32[]{:S(2)}) async-start(), calls=%async_computation.6 | async-start | bytes 7208960 | tf_op jit(solution)/shard_map/all_gather | solution.py:11
  7.3 139.0 %all-gather.6.cloned.1.call-start = ((), (), s32[]{:S(2)}) async-start(), calls=%async_computation.2 | async-start | bytes 1310720 | tf_op jit(solution)/shard_map/all_gather | solution.py:83
  55.9 9.5 %copy-start = (bf16[64,2048]{1,0:T(8,128)(2,1)S(1)}, bf16[64,2048]{1,0:T(8,128)(2,1)}, u32[]{:S(2)}) copy-start(bf16[64,2048]{1,0:T(8,128)(2,1)} %param.14) | copy-start | bytes 786436
  65.4 3.2 copy-start.2
  69.4 185.2 %all-gather.8.cloned.1.call-start = ((), (), s32[]{:S(2)}) async-start(), calls=%async_computation.3 | async-start | bytes 7208960 | tf_op jit(solution)/shard_map/all_gather | solution.py:85
  70.2 290.8 %all-gather.10.cloned.1.call-start = ((), (), s32[]{:S(2)}) async-start(), calls=%async_computation.4 | async-start | bytes 7208960 | tf_op jit(solution)/shard_map/all_gather | solution.py:86
  70.7 322.2 %reduce-scatter.2.cloned.1.call-start = ((), (), s32[]{:S(2)}) async-start(), calls=%async_computation.5 | async-start | bytes 1310720 | tf_op jit(solution)/shard_map/reduce_scatter | solution.py:93
  146.3 214.7 %copy-start.3 = (bf16[256,2048]{1,0:T(8,128)(2,1)S(1)}, bf16[256,2048]{1,0:T(8,128)(2,1)}, u32[]{:S(2)}) copy-start(bf16[256,2048]{1,0:T(8,128)(2,1)} %all-gather.6.cloned.1.call-done) | copy-start | bytes 3145732
Sparse Core Ops, SparseCore 0:
  8.9 119.9 all-gather.11
  130.5 15.7 all-gather.5
  147.9 106.6 all-gather.7
  256.0 104.9 all-gather.9
  369.9 23.0 reduce-scatter.1
